TPU v7x, 32 devices: a whole 2x2x4 slice. The times are simulated.
32 devices in a mesh: sp: 8 (over z, y), tp: 4 (over x, core).
Axes of the slice: x: 2, y: 2, z: 4, core: 2. Of those that a mesh axis runs over, the one named last changes fastest.
Arguments:
- tokens: bfloat16 [2048, 2048], P(('sp', 'tp')), may hold values from -6 to 6
- norm_gain: float32 [2048], replicated, may hold values from 0.1 to 1.9
- query_weight: bfloat16 [1024, 2048], P('tp', 'sp'), may hold values from -0.088609319 to 0.088609319
- key_weight: bfloat16 [256, 2048], P('tp', 'sp'), may hold values from -0.10628699 to 0.10628699
- value_weight: bfloat16 [256, 2048], P('tp', 'sp'), may hold values from -0.125 to 0.125
- gate_weight: bfloat16 [1024, 2048], P('tp', 'sp'), may hold values from -0.125 to 0.125
- left_weight: bfloat16 [1024, 2048], P('tp', 'sp'), may hold values from -0.125 to 0.125
- input_weight: bfloat16 [1024, 2048], P('tp', 'sp'), may hold values from -0.125 to 0.125
- query_gain: float32 [64], replicated, may hold values from 0.3 to 4.5, as said below
- key_gain: float32 [64], replicated, may hold values from 0.3 to 4.5, as said below
- sink_logit: float32 [16], P('tp'), may hold values from 2 to 7
- conv_weight: float32 [3, 1024], P(None, 'tp'), may hold values from -3 to 3
- out_attention: bfloat16 [1024, 2048], P('tp', 'sp'), may hold values from -0.125 to 0.125
- out_conv: bfloat16 [1024, 2048], P('tp', 'sp'), may hold values from -0.125 to 0.125
Outputs:
- mixed: bfloat16 [2048, 2048], P(('sp', 'tp'))
Inputs may be any that keep to these rules, and one draw needn't show every extreme that they name: `query_gain`: positive. `key_gain`: positive.
All inputs are finite; a program needn't handle non-finite values.
Results may differ from a plain program's by a relative error of at most 0.024.
Values may be sent and summed in bfloat16 or wider, within the bound.
A program may use at most 64 MiB of HBM per device.

v0:
```python
import jax
import jax.numpy as jnp
from jax import lax
from jax.sharding import PartitionSpec as P

HEAD_DIM = 64
WINDOW = 128
BLOCK = 128


EPS = 1e-06
ROPE_BASE = 10000.0
NEG_FILL = -1e30


def with_halo(cells, sides, width):
    for axis, dim in sides:
        count = lax.axis_size(axis)
        ends = count - 1
        head = lax.slice_in_dim(cells, 0, width, axis=dim)
        tail = lax.slice_in_dim(cells, cells.shape[dim] - width, cells.shape[dim], axis=dim)
        cells = jnp.concatenate(
            [
                lax.ppermute(tail, axis, [(i, (i + 1) % count) for i in range(ends)]),
                cells,
                lax.ppermute(head, axis, [((i + 1) % count, i) for i in range(ends)]),
            ],
            axis=dim,
        )
    return cells


def normalize(values, gain):
    return values * lax.rsqrt(jnp.mean(values * values, axis=-1, keepdims=True) + EPS) * gain


def rotate(values, positions):
    half = values.shape[-1] // 2
    freq = ROPE_BASE ** (-jnp.arange(half, dtype=jnp.float32) / half)
    angle = positions[:, None] * freq
    cosine = jnp.cos(angle)[:, None, :]
    sine = jnp.sin(angle)[:, None, :]
    first = values[..., :half]
    second = values[..., half:]
    return jnp.concatenate(
        [first * cosine - second * sine, second * cosine + first * sine], axis=-1
    )


def project(rows, weight):
    return lax.dot_general(
        rows, weight, (((1,), (1,)), ((), ())), preferred_element_type=jnp.float32
    ).astype(jnp.bfloat16)


def attend(query_rot, key_rim, value_rim, sinks, offset, total):
    count = query_rot.shape[0]
    local_heads = query_rot.shape[1]
    kv_local = key_rim.shape[1]
    group = local_heads // kv_local
    span = BLOCK + 2 * WINDOW
    nblocks = count // BLOCK
    shaped = query_rot.reshape(nblocks, BLOCK, kv_local, group, HEAD_DIM)
    sink_group = sinks.reshape(kv_local, group)[:, :, None]

    def one_block(packed):
        block_index, query_block = packed
        begin = block_index * BLOCK
        key_block = lax.dynamic_slice_in_dim(key_rim, begin, span, 0)
        value_block = lax.dynamic_slice_in_dim(value_rim, begin, span, 0)
        scores = jnp.einsum(
            "qkgd,nkd->kgqn", query_block, key_block, preferred_element_type=jnp.float32
        ) * HEAD_DIM ** (-0.5)
        query_pos = offset + begin + jnp.arange(BLOCK, dtype=jnp.int32)
        key_pos = offset + begin - WINDOW + jnp.arange(span, dtype=jnp.int32)
        allowed = (
            (jnp.abs(query_pos[:, None] - key_pos[None, :]) <= WINDOW)
            & (key_pos >= 0)[None, :]
            & (key_pos < total)[None, :]
        )
        scores = jnp.where(allowed, scores, NEG_FILL)
        top = jnp.maximum(jnp.max(scores, axis=-1), sink_group)
        expo = jnp.exp(scores - top[..., None])
        denom = jnp.sum(expo, axis=-1) + jnp.exp(sink_group - top)
        weights = (expo / denom[..., None]).astype(jnp.bfloat16)
        return jnp.einsum(
            "kgqn,nkd->qkgd", weights, value_block, preferred_element_type=jnp.float32
        ).astype(jnp.bfloat16)

    result = lax.map(one_block, (jnp.arange(nblocks, dtype=jnp.int32), shaped))
    return result.reshape(count, local_heads * HEAD_DIM)


def per_device(
    tokens,
    norm_gain,
    query_weight,
    key_weight,
    value_weight,
    gate_weight,
    left_weight,
    input_weight,
    query_gain,
    key_gain,
    sink_logit,
    conv_weight,
    out_attention,
    out_conv,
):
    sp_count = lax.axis_size("sp")
    sp_place = lax.axis_index("sp")
    gathered = (
        lax.all_gather(query_weight, "sp", axis=1, tiled=True),
        lax.all_gather(key_weight, "sp", axis=1, tiled=True),
        lax.all_gather(value_weight, "sp", axis=1, tiled=True),
        lax.all_gather(gate_weight, "sp", axis=1, tiled=True),
        lax.all_gather(left_weight, "sp", axis=1, tiled=True),
        lax.all_gather(input_weight, "sp", axis=1, tiled=True),
        lax.all_gather(out_attention, "sp", axis=1, tiled=True),
        lax.all_gather(out_conv, "sp", axis=1, tiled=True),
    )
    (
        query_full,
        key_full,
        value_full,
        gate_full,
        left_full,
        input_full,
        attn_out_full,
        conv_out_full,
    ) = gathered
    normed = normalize(tokens.astype(jnp.float32), norm_gain).astype(jnp.bfloat16)
    widths = [
        query_full.shape[0],
        key_full.shape[0],
        value_full.shape[0],
        gate_full.shape[0],
        left_full.shape[0],
        input_full.shape[0],
    ]
    piece = lax.all_gather(normed, "tp", axis=0, tiled=True)
    joined = jnp.concatenate(
        [
            project(piece, weight)
            for weight in (query_full, key_full, value_full, gate_full, left_full, input_full)
        ],
        axis=1,
    )
    count = joined.shape[0]
    bounds = [0]
    for width in widths:
        bounds.append(bounds[-1] + width)
    query, keys, values, gate, left, inputs = [
        joined[:, bounds[place] : bounds[place + 1]] for place in range(6)
    ]
    offset = sp_place * count
    total = count * sp_count
    positions = (offset + jnp.arange(count, dtype=jnp.int32)).astype(jnp.float32)
    local_heads = widths[0] // HEAD_DIM
    kv_local = widths[1] // HEAD_DIM
    query_rot = rotate(
        normalize(query.reshape(count, local_heads, HEAD_DIM).astype(jnp.float32), query_gain),
        positions,
    ).astype(jnp.bfloat16)
    key_rot = rotate(
        normalize(keys.reshape(count, kv_local, HEAD_DIM).astype(jnp.float32), key_gain), positions
    ).astype(jnp.bfloat16)
    key_flat = key_rot.reshape(count, kv_local * HEAD_DIM)
    product = (left.astype(jnp.float32) * inputs.astype(jnp.float32)).astype(jnp.bfloat16)
    kv_width = widths[1]
    pair_rim = with_halo(jnp.concatenate([key_flat, values], axis=1), (("sp", 0),), WINDOW)
    product_rim = with_halo(product, (("sp", 0),), 1)
    rim_rows = pair_rim.shape[0]
    key_rim = pair_rim[:, :kv_width].reshape(rim_rows, kv_local, HEAD_DIM)
    value_rim = pair_rim[:, kv_width:].reshape(rim_rows, kv_local, HEAD_DIM)
    attended = attend(query_rot, key_rim, value_rim, sink_logit, offset, total)
    padded = product_rim.astype(jnp.float32)
    convolved = (
        conv_weight[0] * padded[:-2] + conv_weight[1] * padded[1:-1] + conv_weight[2] * padded[2:]
    )
    gated = (gate.astype(jnp.float32) * convolved).astype(jnp.bfloat16)
    return lax.psum_scatter(
        (
            jnp.dot(attended, attn_out_full, preferred_element_type=jnp.float32)
            + jnp.dot(gated, conv_out_full, preferred_element_type=jnp.float32)
        ).astype(jnp.bfloat16),
        "tp",
        scatter_dimension=0,
        tiled=True,
    )


def solution(mesh):
    in_specs = (
        P(("sp", "tp"), None),
        P(),
        P("tp", "sp"),
        P("tp", "sp"),
        P("tp", "sp"),
        P("tp", "sp"),
        P("tp", "sp"),
        P("tp", "sp"),
        P(),
        P(),
        P("tp"),
        P(None, "tp"),
        P("tp", "sp"),
        P("tp", "sp"),
    )
    out_specs = P(("sp", "tp"), None)
    return jax.shard_map(
        per_device, mesh=mesh, in_specs=in_specs, out_specs=out_specs, check_vma=False
    )
```

profile of v0, /device:TPU:0, one launch (start us, length us, event | category | flops | bytes accessed | tf_op | source)
XLA Modules:
  0.0 308.3 jit_solution(10215784313239351331)
XLA Ops:
  6.5 1.1 fusion.27
  7.7 1.8 fusion.29
  9.5 0.7 all-gather.10.cloned.1.call-update
  10.3 0.7 all-gather.16.cloned.1.call-update
  11.0 0.5 all-gather.18.cloned.1.call-update
  11.6 0.5 all-gather.12.cloned.1.call-update
  12.2 0.5 all-gather.14.cloned.1.call-update
  12.8 0.7 all-gather.20.cloned.1.call-update
  13.6 32.9 %all_gather.28 = bf16[64,2048]{1,0:T(8,128)(2,1)S(1)} all-gather(bf16[64,256]{1,0:T(8,128)(2,1)} %param.19), channel_id=1, replica_groups=mesh['sp'=8,'tp'=4] {'sp'}, dimensions={1}, use_global_device_ids=true | all-gather | bytes 294912 | tf_op jit(solution)/shard_map/all_gather | solution.py:114
  46.5 31.3 %all_gather.29 = bf16[64,2048]{1,0:T(8,128)(2,1)S(1)} all-gather(bf16[64,256]{1,0:T(8,128)(2,1)S(1)} %copy-done.2), channel_id=1, replica_groups=mesh['sp'=8,'tp'=4] {'sp'}, dimensions={1}, use_global_device_ids=true | all-gather | bytes 294912 | tf_op jit(solution)/shard_map/all_gather | solution.py:115
  77.8 0.2 multiply_cosine_fusion
  78.0 1.8 multiply_reduce_fusion
  79.8 0.1 multiply_bitcast_fusion
  79.9 0.2 fusion.51
  80.1 1.7 convolution_convert_fusion.5
  81.8 3.3 %collective-permute-start = (bf16[128,128]{0,1:T(8,128)(2,1)S(1)}, bf16[128,128]{0,1:T(8,128)(2,1)S(1)}, u32[]{:S(2)}, u32[]{:S(2)}) collective-permute-start(bf16[128,128]{0,1:T(8,128)(2,1)S(1)} %get-tuple-element.143), channel_id=1, source_target_pairs={{0,4},{4,8},{8,12},{12,16},{16,20},{20,24},{24,28},{1,5},{5,9},{9,... | collective-permute-start | bytes 98312 | tf_op jit(solution)/shard_map/ppermute | solution.py:24
  85.1 1.3 collective-permute-start.1
  86.4 0.5 fusion.55
  87.0 4.0 %collective-permute-done.1 = bf16[128,128]{0,1:T(8,128)(2,1)S(1)} collective-permute-done((bf16[128,128]{0,1:T(8,128)(2,1)S(1)}, bf16[128,128]{0,1:T(8,128)(2,1)S(1)}, u32[]{:S(2)}, u32[]{:S(2)}) %collective-permute-start.1) | collective-permute-done | bytes 32800 | tf_op jit(solution)/shard_map/ppermute | solution.py:26
  91.0 1.7 fusion.30
  92.7 0.1 fusion.31
  92.9 0.2 pad_maximum_fusion.1
  93.2 4.8 %while.12 = (s32[]{:T(128)}, bf16[2,128,1,4,64]{1,4,3,2,0:T(8,128)(2,1)S(1)}, s32[2]{0:T(128)S(1)}, bf16[512,1,64]{0,2,1:T(8,128)(2,1)S(1)}, s32[]{:T(128)}, /*i...) while((s32[]{:T(128)}, ...), condition=%wide.region_6.7_spmd, body=%wide.region_3.6_spmd.sunk | while | flops 52185736 | bytes 2713355 | solution.py:90
  93.2 0.6 dynamic_slice.49
  94.4 0.2 fusion.80
  94.7 0.3 fusion.81
  95.0 0.1 fusion.82
  95.3 0.3 fusion.83
  95.6 0.6 dynamic_slice.49
  96.8 0.2 fusion.80
  97.0 0.3 fusion.81
  97.4 0.1 fusion.82
  97.6 0.3 fusion.83
  97.9 0.1 copy.18
  98.1 14.0 %all-gather.16.cloned.1.call-done = bf16[256,2048]{1,0:T(8,128)(2,1)} async-done(((bf16[256,256]{1,0:T(8,128)(2,1)}), bf16[256,2048]{1,0:T(8,128)(2,1)}) %all-gather.16.cloned.1.call-update) | async-done | bytes 1048592 | tf_op jit(solution)/shard_map/all_gather | solution.py:117
  112.1 1.7 fusion.22
  113.8 38.6 %all-gather.18.cloned.1.call-done = bf16[256,2048]{1,0:T(8,128)(2,1)} async-done(((bf16[256,256]{1,0:T(8,128)(2,1)}), bf16[256,2048]{1,0:T(8,128)(2,1)}) %all-gather.18.cloned.1.call-update) | async-done | bytes 1048592 | tf_op jit(solution)/shard_map/all_gather | solution.py:118
  152.4 1.7 fusion.21
  154.1 2.9 collective-permute-start.2
  157.1 1.3 collective-permute-start.3
  158.4 34.4 %all-gather.12.cloned.1.call-done = bf16[256,2048]{1,0:T(8,128)(2,1)} async-done(((bf16[256,256]{1,0:T(8,128)(2,1)}), bf16[256,2048]{1,0:T(8,128)(2,1)}) %all-gather.12.cloned.1.call-update) | async-done | bytes 1048592 | tf_op jit(solution)/shard_map/all_gather | solution.py:119
  192.8 1.7 fusion.36
  194.5 0.6 copy-done.4
  195.0 0.7 maximum_convert_fusion
  195.7 37.4 %all-gather.14.cloned.1.call-done = bf16[256,2048]{1,0:T(8,128)(2,1)} async-done(((bf16[256,256]{1,0:T(8,128)(2,1)}), bf16[256,2048]{1,0:T(8,128)(2,1)}) %all-gather.14.cloned.1.call-update) | async-done | bytes 1048592 | tf_op jit(solution)/shard_map/all_gather | solution.py:116
  233.1 40.5 %all-gather.20.cloned.1.call-done = bf16[256,2048]{1,0:T(8,128)(2,1)} async-done(((bf16[256,256]{1,0:T(8,128)(2,1)}), bf16[256,2048]{1,0:T(8,128)(2,1)}) %all-gather.20.cloned.1.call-update) | async-done | bytes 1048592 | tf_op jit(solution)/shard_map/all_gather | solution.py:120
  273.6 3.9 %fusion.18 = bf16[256,2048]{1,0:T(8,128)(2,1)} fusion(f32[256,2048]{1,0:T(8,128)S(1)} %fusion.36, bf16[256,2048]{1,0:T(8,128)(2,1)} %all-gather.20.cloned.1.call-done, bf16[256,2048]{1,0:T(8,128)(2,1)S(1)} %copy-done, bf16[256,2048]{1,0:T(8,128)(2,1)} %all-gather.14.cloned.1.call-done, f32[258,256]{1,0:T(8,128)S(1)} %maximum_convert_fusion, ...), kind=kOutput, calls=%fused_computation.28 | convolution fusion | flops 538509312 | bytes 7080960 | tf_op jit(solution)/shard_map/dot_general | solution.py:185
  277.5 24.0 %reduce-scatter.2.cloned.1.call-done = bf16[64,2048]{1,0:T(8,128)(2,1)} async-done(((bf16[256,2048]{1,0:T(8,128)(2,1)}), bf16[64,2048]{1,0:T(8,128)(2,1)}) %reduce-scatter.2.cloned.1.call-update) | async-done | bytes 262160 | tf_op jit(solution)/shard_map/reduce_scatter | solution.py:182
  (54 shorter events, 0.9 us)
Async XLA Ops:
  6.5 39.9 %copy-start.2 = (bf16[64,256]{1,0:T(8,128)(2,1)S(1)}, bf16[64,256]{1,0:T(8,128)(2,1)}, u32[]{:S(2)}) copy-start(bf16[64,256]{1,0:T(8,128)(2,1)} %param.20) | copy-start | bytes 98308
  6.5 73.3 %copy-start.5 = (f32[64]{0:T(128)S(1)}, f32[64]{0:T(128)}, u32[]{:S(2)}) copy-start(f32[64]{0:T(128)} %param.25) | copy-start | bytes 772
  6.5 71.5 %all-gather.8.cloned.1.call-start = ((), (), s32[]{:S(2)}) async-start(), calls=%async_computation.1 | async-start | bytes 1310720 | tf_op jit(solution)/shard_map/all_gather | solution.py:141
  9.5 81.5 %all-gather.10.cloned.1.call-start = ((), (), s32[]{:S(2)}) async-start(), calls=%async_computation.2 | async-start | bytes 1179648 | tf_op jit(solution)/shard_map/all_gather | solution.py:113
  10.3 101.9 %all-gather.16.cloned.1.call-start = ((), (), s32[]{:S(2)}) async-start(), calls=%async_computation.5 | async-start | bytes 1179648 | tf_op jit(solution)/shard_map/all_gather | solution.py:117
  11.0 141.4 %all-gather.18.cloned.1.call-start = ((), (), s32[]{:S(2)}) async-start(), calls=%async_computation.6 | async-start | bytes 1179648 | tf_op jit(solution)/shard_map/all_gather | solution.py:118
  11.6 181.2 %all-gather.12.cloned.1.call-start = ((), (), s32[]{:S(2)}) async-start(), calls=%async_computation.3 | async-start | bytes 1179648 | tf_op jit(solution)/shard_map/all_gather | solution.py:119
  12.2 74.3 %copy-start.3 = (f32[3,256]{1,0:T(4,128)S(1)}, f32[3,256]{1,0:T(4,128)}, u32[]{:S(2)}) copy-start(f32[3,256]{1,0:T(4,128)} %param.27) | copy-start | bytes 9220
  12.2 220.9 %all-gather.14.cloned.1.call-start = ((), (), s32[]{:S(2)}) async-start(), calls=%async_computation.4 | async-start | bytes 1179648 | tf_op jit(solution)/shard_map/all_gather | solution.py:116
  12.7 260.9 %all-gather.20.cloned.1.call-start = ((), (), s32[]{:S(2)}) async-start(), calls=%async_computation.7 | async-start | bytes 1179648 | tf_op jit(solution)/shard_map/all_gather | solution.py:120
  13.5 287.9 %reduce-scatter.2.cloned.1.call-start = ((), (), s32[]{:S(2)}) async-start(), calls=%async_computation.8 | async-start | bytes 1310720 | tf_op jit(solution)/shard_map/reduce_scatter | solution.py:182
  78.0 13.0 %copy-start = (bf16[256,2048]{1,0:T(8,128)(2,1)S(1)}, bf16[256,2048]{1,0:T(8,128)(2,1)}, u32[]{:S(2)}) copy-start(bf16[256,2048]{1,0:T(8,128)(2,1)} %all-gather.8.cloned.1.call-done) | copy-start | bytes 3145732
  80.1 12.6 %copy-start.6 = (f32[64]{0:T(128)S(1)}, f32[64]{0:T(128)}, u32[]{:S(2)}) copy-start(f32[64]{0:T(128)} %param.24) | copy-start | bytes 772
  81.8 5.1 %collective-permute-start = (bf16[128,128]{0,1:T(8,128)(2,1)S(1)}, bf16[128,128]{0,1:T(8,128)(2,1)S(1)}, u32[]{:S(2)}, u32[]{:S(2)}) collective-permute-start(bf16[128,128]{0,1:T(8,128)(2,1)S(1)} %get-tuple-element.143), channel_id=1, source_target_pairs={{0,4},{4,8},{8,12},{12,16},{16,20},{20,24},{24,28},{1,5},{5,9},{9,... | collective-permute-start | bytes 98312 | tf_op jit(solution)/shard_map/ppermute | solution.py:24
  85.1 5.8 %collective-permute-start.1 = (bf16[128,128]{0,1:T(8,128)(2,1)S(1)}, bf16[128,128]{0,1:T(8,128)(2,1)S(1)}, u32[]{:S(2)}, u32[]{:S(2)}) collective-permute-start(bf16[128,128]{0,1:T(8,128)(2,1)S(1)} %get-tuple-element.144), channel_id=1, source_target_pairs={{4,0},{8,4},{12,8},{16,12},{20,16},{24,20},{28,24},{5,1},{9,5},{13... | collective-permute-start | bytes 98312 | tf_op jit(solution)/shard_map/ppermute | solution.py:26
  90.9 2.2 copy-start.1
  154.1 40.3 %collective-permute-start.2 = (bf16[1,256]{1,0:T(2,128)(2,1)S(1)}, bf16[1,256]{1,0:T(2,128)(2,1)S(1)}, u32[]{:S(2)}, u32[]{:S(2)}) collective-permute-start(bf16[1,256]{1,0:T(2,128)(2,1)S(1)} %get-tuple-element.137), channel_id=1, source_target_pairs={{0,4},{4,8},{8,12},{12,16},{16,20},{20,24},{24,28},{1,5},{5,9},{9,... | collective-permute-start | bytes 1544 | tf_op jit(solution)/shard_map/ppermute | solution.py:24
  157.1 37.9 %collective-permute-start.3 = (bf16[1,256]{1,0:T(2,128)(2,1)S(1)}, bf16[1,256]{1,0:T(2,128)(2,1)}, u32[]{:S(2)}, u32[]{:S(2)}) collective-permute-start(bf16[1,256]{1,0:T(2,128)(2,1)S(1)} %get-tuple-element.138), channel_id=1, source_target_pairs={{4,0},{8,4},{12,8},{16,12},{20,16},{24,20},{28,24},{5,1},{9,5},{13... | collective-permute-start | bytes 1544 | tf_op jit(solution)/shard_map/ppermute | solution.py:26
  194.5 0.6 copy-start.4
Sparse Core Ops, SparseCore 0:
  9.6 19.4 all-gather.7
  31.1 40.8 all-gather.9
  74.0 38.0 all-gather.15
  114.0 38.3 all-gather.17
  154.3 38.3 all-gather.11
  194.7 38.3 all-gather.13
  235.1 38.3 all-gather.19
  277.6 23.7 reduce-scatter.1
where the time goes:
time: 309 us; the launch traced here: 308 us
  waiting for transfers between devices  197 us (64%)
  blocking collectives  64.2 us (21%)
  matrix products  15.3 us (5%)
  between operations  13.8 us (4%)
  starting transfers between devices  9.06 us (3%)
  other arithmetic  5.49 us (2%)
    all_gather x1, waiting for transfers between devices, per_device(): lax.all_gather(out_conv, 'sp', axis=1, tiled=True)  40.5 us
    all_gather x1, waiting for transfers between devices, per_device(): lax.all_gather(input_weight, 'sp', axis=1, tiled=True)  38.6 us
    all_gather x1, waiting for transfers between devices, per_device(): lax.all_gather(gate_weight, 'sp', axis=1, tiled=True)  37.4 us
    all_gather x1, waiting for transfers between devices, per_device(): lax.all_gather(out_attention, 'sp', axis=1, tiled=True)  34.4 us
    all_gather x1, blocking collectives, per_device(): lax.all_gather(key_weight, 'sp', axis=1, tiled=True)  32.9 us
    all_gather x1, blocking collectives, per_device(): lax.all_gather(value_weight, 'sp', axis=1, tiled=True)  31.3 us
    reduce_scatter x1, waiting for transfers between devices, per_device(): lax.psum_scatter((jnp.dot(attended, attn_out_full, preferred_element_type...  24 us
    all_gather x1, waiting for transfers between devices, per_device(): lax.all_gather(left_weight, 'sp', axis=1, tiled=True)  14 us
  transfers between devices with their start and end apart: 12, of which 7 were waited for; matrix products, arithmetic and copies ran while one was open for 5% of the time, Pallas kernels for 0%

commit v1 on v0

--- a/solution.py
+++ b/solution.py
@@ -1,6 +1,11 @@
+import functools
+
 import jax
 import jax.numpy as jnp
+import numpy as np
 from jax import lax
+from jax.experimental import pallas as pl
+from jax.experimental.pallas import tpu as pltpu
 from jax.sharding import PartitionSpec as P
 
 HEAD_DIM = 64
@@ -190,6 +195,518 @@
     )
 
 
+MESH = pl.DeviceIdType.MESH
+
+
+def fused_kernel(
+    dims,
+    tok_hbm, gain_ref, q_hbm, k_hbm, v_hbm, g_hbm, l_hbm, i_hbm,
+    qgain_ref, kgain_ref, sink_ref, conv_ref, oa_hbm, oc_hbm, trig_hbm,
+    out_ref,
+    tok, trig, stage, ostage, win, wout, normed, acc, rim, mix, qrot,
+    keep, s1, r1, s2, r2, s3, r3,
+    local_sem, y_send, oy_send, in_recv, out_recv, in_up, in_down, out_up, out_down,
+    tok_send, tok_recv, rim_send, rim_recv, rs_send, rs_recv,
+):
+    line, rows, depth, qr, kr, cr = (
+        dims["line"], dims["rows"], dims["depth"], dims["qr"], dims["kr"], dims["cr"]
+    )
+    sp = lax.axis_index("sp")
+    tp = lax.axis_index("tp")
+    z, y = sp // 2, sp % 2
+    x, c = tp // 2, tp % 2
+    y_peer = (2 * z + 1 - y, tp)
+    x_peer = (sp, 2 * (1 - x) + c)
+    c_peer = (sp, 2 * x + 1 - c)
+    up = (jnp.minimum(2 * (z + 1) + y, 2 * line - 1), tp)
+    down = (jnp.maximum(2 * (z - 1) + y, 0), tp)
+    has_up = z < line - 1
+    has_down = z > 0
+    s_own = sp
+    s_mate = 2 * z + 1 - y
+    plane = 8 * rows
+
+    barrier = pltpu.get_barrier_semaphore()
+    for peer in (y_peer, x_peer, c_peer):
+        pl.semaphore_signal(barrier, inc=1, device_id=peer, device_id_type=MESH)
+
+    @pl.when(has_up)
+    def _():
+        pl.semaphore_signal(barrier, inc=1, device_id=up, device_id_type=MESH)
+
+    @pl.when(has_down)
+    def _():
+        pl.semaphore_signal(barrier, inc=1, device_id=down, device_id_type=MESH)
+
+    counter = [0]
+
+    def local(src, dst):
+        copy = pltpu.make_async_copy(src, dst, local_sem.at[counter[0]])
+        counter[0] += 1
+        copy.start()
+        return copy
+
+    def pieces(which, dst):
+        q0, c0 = pl.multiple_of(which * qr, qr), pl.multiple_of(which * cr, cr)
+        return [
+            local(q_hbm.at[pl.ds(q0, qr)], dst.at[0:qr]),
+            local(k_hbm, dst.at[qr : qr + kr]),
+            local(v_hbm, dst.at[qr + kr : qr + 2 * kr]),
+            local(g_hbm.at[pl.ds(c0, cr)], dst.at[qr + 2 * kr : qr + 2 * kr + cr]),
+            local(l_hbm.at[pl.ds(c0, cr)], dst.at[qr + 2 * kr + cr : qr + 2 * kr + 2 * cr]),
+            local(i_hbm.at[pl.ds(c0, cr)], dst.at[qr + 2 * kr + 2 * cr : qr + 2 * kr + 3 * cr]),
+        ]
+
+    def out_pieces(which, dst):
+        q0, c0 = pl.multiple_of(which * qr, qr), pl.multiple_of(which * cr, cr)
+        return [
+            local(oa_hbm.at[pl.ds(q0, qr)], dst.at[0:qr]),
+            local(oc_hbm.at[pl.ds(c0, cr)], dst.at[qr : qr + cr]),
+        ]
+
+    mine = pieces(y, win.at[s_own])
+    theirs = pieces(1 - y, stage)
+    tok_copy = local(tok_hbm, tok)
+    out_theirs = out_pieces(1 - y, ostage)
+    out_mine = out_pieces(y, wout.at[s_own])
+    trig_copy = local(trig_hbm.at[pl.ds(pl.multiple_of(z * plane, plane), plane)], trig)
+
+    pl.semaphore_wait(barrier, 3 + has_up.astype(jnp.int32) + has_down.astype(jnp.int32))
+
+    def remote(src, dst, send, recv, peer):
+        return pltpu.make_async_remote_copy(
+            src_ref=src, dst_ref=dst, send_sem=send, recv_sem=recv,
+            device_id=peer, device_id_type=MESH,
+        )
+
+    def hop(buf, s, send, recv, peer):
+        return remote(buf.at[s], buf.at[s], send.at[s], recv.at[s], peer)
+
+    def forward(buf, s, source, ups, downs, recv):
+        @pl.when((source <= z) & has_up)
+        def _():
+            hop(buf, s, ups, recv, up).start()
+
+        @pl.when((source >= z) & has_down)
+        def _():
+            hop(buf, s, downs, recv, down).start()
+
+    for copy in mine:
+        copy.wait()
+    forward(win, s_own, z, in_up, in_down, in_recv)
+    for copy in theirs:
+        copy.wait()
+    y_copy = remote(stage, win.at[s_own], y_send.at[0], in_recv.at[s_own], y_peer)
+    y_copy.start()
+    tok_copy.wait()
+    t = tok[...].astype(jnp.float32)
+    t = t * lax.rsqrt(jnp.mean(t * t, axis=-1, keepdims=True) + EPS) * gain_ref[...]
+    own_block = 4 * y + 2 * x + c
+    normed[own_block] = t.astype(jnp.bfloat16)
+    for copy in out_theirs:
+        copy.wait()
+    oy_copy = remote(ostage, wout.at[s_own], oy_send.at[0], out_recv.at[s_own], y_peer)
+    oy_copy.start()
+    for copy in out_mine:
+        copy.wait()
+
+    def block_of(yy, xx, cc):
+        return 4 * yy + 2 * xx + cc
+
+    def tok_hop(block, slot, peer):
+        return remote(
+            normed.at[block], normed.at[block], tok_send.at[slot], tok_recv.at[block], peer
+        )
+
+    xb = block_of(y, 1 - x, c)
+    yb0 = block_of(1 - y, x, c)
+    yb1 = block_of(1 - y, 1 - x, c)
+    tok_copies = [
+        tok_hop(own_block, 0, x_peer),
+        tok_hop(own_block, 1, y_peer),
+        tok_hop(own_block, 2, c_peer),
+    ]
+    for copy in tok_copies:
+        copy.start()
+
+    def tok_wait(block):
+        tok_hop(block, 0, x_peer).wait_recv()
+
+    tok_wait(xb)
+    more = [tok_hop(xb, 3, y_peer), tok_hop(xb, 4, c_peer)]
+    for copy in more:
+        copy.start()
+    tok_copies += more
+
+    hop(win, s_mate, in_up, in_recv, up).wait_recv()
+    forward(win, s_mate, z, in_up, in_down, in_recv)
+    hop(wout, s_mate, out_up, out_recv, up).wait_recv()
+
+    def own_out(flag_up, flag_down):
+        for s in (s_own, s_mate):
+            @pl.when(flag_up & has_up)
+            def _():
+                hop(wout, s, out_up, out_recv, up).start()
+
+            @pl.when(flag_down & has_down)
+            def _():
+                hop(wout, s, out_down, out_recv, down).start()
+
+    own_out(z == 0, z == line - 1)
+
+    tok_wait(yb0)
+    copy = tok_hop(yb0, 5, c_peer)
+    copy.start()
+    tok_copies.append(copy)
+    tok_wait(yb1)
+    copy = tok_hop(yb1, 6, c_peer)
+    copy.start()
+    tok_copies.append(copy)
+    for yy in range(2):
+        for xx in range(2):
+            tok_wait(block_of(yy, xx, 1 - c))
+
+    def columns(s):
+        return pl.ds(pl.multiple_of(s * depth, depth), depth)
+
+    def in_dot(s):
+        a = normed[:, :, columns(s)].reshape(plane, depth)
+        return lax.dot_general(
+            a, win[s], (((1,), (1,)), ((), ())), preferred_element_type=jnp.float32
+        )
+
+    paired = jnp.minimum(z, line - 1 - z)
+    below_longer = z > line - 1 - z
+
+    def source_of(k):
+        d = jnp.where(k <= 2 * paired, (k + 1) // 2, k - paired)
+        below = jnp.where(k <= 2 * paired, k % 2 == 1, below_longer)
+        return jnp.where(below, z - d, z + d)
+
+    acc[...] = in_dot(s_own)
+    acc[...] += in_dot(s_mate)
+
+    def in_step(k, carry):
+        source = source_of(k)
+        for half in range(2):
+            first = jnp.where(half == 0, y, 1 - y)
+            s = 2 * source + first
+            hop(win, s, in_up, in_recv, up).wait_recv()
+            forward(win, s, source, in_up, in_down, in_recv)
+            if half == 1:
+                own_out(source == 0, source == line - 1)
+            acc[...] += in_dot(s)
+        return carry
+
+    lax.fori_loop(1, line, in_step, 0)
+
+    trig_copy.wait()
+    lane = lax.broadcasted_iota(jnp.int32, (plane, qr), 1)
+    half_dim = HEAD_DIM // 2
+    table = trig[...]
+    cos2 = jnp.where(lane < HEAD_DIM, table, pltpu.roll(table, HEAD_DIM, 1))
+    sin2 = jnp.where(lane < HEAD_DIM, pltpu.roll(table, HEAD_DIM, 1), table)
+    low = lane < HEAD_DIM
+    first_half = lane % HEAD_DIM < half_dim
+
+    def rot(v):
+        partner = jnp.where(
+            first_half, pltpu.roll(v, qr - half_dim, 1), pltpu.roll(v, half_dim, 1)
+        )
+        return v * cos2 + partner * sin2
+
+    def bf(v):
+        return v.astype(jnp.bfloat16).astype(jnp.float32)
+
+    kv = bf(acc[:, qr : 2 * qr])
+    ksq = jnp.sum(jnp.where(low, kv * kv, 0.0), axis=-1, keepdims=True) / HEAD_DIM
+    kn = kv * lax.rsqrt(ksq + EPS) * kgain_ref[...]
+    krot = rot(kn)
+    rim[WINDOW : WINDOW + plane, 0:qr] = jnp.where(low, krot, kv).astype(jnp.bfloat16)
+    base = 2 * qr
+    left = bf(acc[:, base + cr : base + 2 * cr])
+    inputs = bf(acc[:, base + 2 * cr : base + 3 * cr])
+    rim[WINDOW : WINDOW + plane, qr : qr + cr] = (left * inputs).astype(jnp.bfloat16)
+
+    qv = bf(acc[:, 0:qr])
+    qq = qv * qv
+    q_lo = jnp.sum(jnp.where(low, qq, 0.0), axis=-1, keepdims=True) / HEAD_DIM
+    q_hi = jnp.sum(jnp.where(low, 0.0, qq), axis=-1, keepdims=True) / HEAD_DIM
+    qn = qv * lax.rsqrt(jnp.where(low, q_lo, q_hi) + EPS) * qgain_ref[...]
+    qro = rot(qn)
+
+    bottom = pl.ds(WINDOW, WINDOW)
+    top = pl.ds(plane, WINDOW)
+    rim_up = remote(rim.at[top], rim.at[pl.ds(0, WINDOW)], rim_send.at[0], rim_recv.at[0], up)
+    rim_down = remote(
+        rim.at[bottom], rim.at[pl.ds(WINDOW + plane, WINDOW)], rim_send.at[1], rim_recv.at[1], down
+    )
+
+    @pl.when(has_up)
+    def _():
+        rim_up.start()
+
+    @pl.when(has_down)
+    def _():
+        rim_down.start()
+
+    zero_rim = jnp.zeros((WINDOW, qr + cr), jnp.bfloat16)
+
+    @pl.when(z == 0)
+    def _():
+        rim[0:WINDOW] = zero_rim
+
+    @pl.when(z == line - 1)
+    def _():
+        rim[WINDOW + plane :] = zero_rim
+
+    qrot[0] = jnp.where(low, qro, 0.0).astype(jnp.bfloat16)
+    qrot[1] = jnp.where(low, pltpu.roll(qro, HEAD_DIM, 1), 0.0).astype(jnp.bfloat16)
+
+    @pl.when(has_down)
+    def _():
+        rim_up.wait_recv()
+
+    @pl.when(has_up)
+    def _():
+        rim_down.wait_recv()
+
+    span = BLOCK + 2 * WINDOW
+    total = plane * line
+
+    def att_step(block, carry):
+        begin = pl.multiple_of(block * BLOCK, BLOCK)
+        kvb = rim[pl.ds(begin, span), 0:qr]
+        qb = qrot[:, pl.ds(begin, BLOCK), :].reshape(2 * BLOCK, qr)
+        scores = lax.dot_general(
+            qb, kvb, (((1,), (1,)), ((), ())), preferred_element_type=jnp.float32
+        ) * HEAD_DIM ** (-0.5)
+        row = lax.broadcasted_iota(jnp.int32, (2 * BLOCK, span), 0)
+        col = lax.broadcasted_iota(jnp.int32, (2 * BLOCK, span), 1)
+        gap = row % BLOCK + WINDOW - col
+        pos = z * plane + begin - WINDOW + col
+        allowed = (gap <= WINDOW) & (gap >= -WINDOW) & (pos >= 0) & (pos < total)
+        scores = jnp.where(allowed, scores, NEG_FILL)
+        head = lax.broadcasted_iota(jnp.int32, (2 * BLOCK, 1), 0)
+        sink = jnp.where(head < BLOCK, sink_ref[0, 2 * y], sink_ref[0, 2 * y + 1])
+        peak = jnp.maximum(jnp.max(scores, axis=-1, keepdims=True), sink)
+        expo = jnp.exp(scores - peak)
+        denom = jnp.sum(expo, axis=-1, keepdims=True) + jnp.exp(sink - peak)
+        weights = (expo / denom).astype(jnp.bfloat16)
+        o = jnp.dot(weights, kvb, preferred_element_type=jnp.float32)
+        low_b = lax.broadcasted_iota(jnp.int32, (BLOCK, qr), 1) < HEAD_DIM
+        both = jnp.where(low_b, pltpu.roll(o[:BLOCK], HEAD_DIM, 1), o[BLOCK:])
+        mix[pl.ds(begin, BLOCK), 0:qr] = both.astype(jnp.bfloat16)
+        return carry
+
+    lax.fori_loop(0, plane // BLOCK, att_step, 0)
+
+    extra = plane + 32
+    p = rim[WINDOW - 16 : WINDOW + plane + 16, qr : qr + cr].astype(jnp.float32)
+    taps = conv_ref[y]
+    before = pltpu.roll(p, 1, 0)[16 : 16 + plane]
+    after = pltpu.roll(p, extra - 1, 0)[16 : 16 + plane]
+    convolved = taps[0:1] * before + taps[1:2] * p[16 : 16 + plane] + taps[2:3] * after
+    gate = bf(acc[:, base : base + cr])
+    mix[:, qr : qr + cr] = (gate * convolved).astype(jnp.bfloat16)
+
+    def group(cc):
+        return [
+            mix[pl.ds(pl.multiple_of((2 * q + cc) * rows, rows), rows), :] for q in range(4)
+        ]
+
+    mine_rows = jnp.concatenate(group(c), axis=0)
+    other_rows = jnp.concatenate(group(1 - c), axis=0)
+    rs_copies = []
+
+    def send_rs(src, dst, stage_id, s, peer):
+        copy = remote(src, dst, rs_send.at[stage_id, s], rs_recv.at[stage_id, s], peer)
+        copy.start()
+        rs_copies.append(copy)
+
+    def stage_a(k):
+        source = z if k == 0 else source_of(jnp.int32(k))
+        for half in range(2):
+            s = 2 * source + half
+            if k:
+                hop(wout, s, out_up, out_recv, up).wait_recv()
+                forward(wout, s, source, out_up, out_down, out_recv)
+            weight = wout[s]
+            s1[s] = jnp.dot(
+                other_rows, weight, preferred_element_type=jnp.float32
+            ).astype(jnp.bfloat16).reshape(2, 2, rows, depth)
+            send_rs(s1.at[s], r1.at[s], 0, s, c_peer)
+            keep[s] = jnp.dot(
+                mine_rows, weight, preferred_element_type=jnp.float32
+            ).reshape(2, 2, rows, depth)
+
+    def axis_index_of(half):
+        return (y, x) if half == 0 else (x, y)
+
+    def stage_b(k):
+        source = z if k == 0 else source_of(jnp.int32(k))
+        for half in range(2):
+            s = 2 * source + half
+            remote(s1.at[s], r1.at[s], rs_send.at[0, s], rs_recv.at[0, s], c_peer).wait_recv()
+            for j in range(2):
+                if half == 0:
+                    s2[s, j] = (keep[s, 1 - y, j] + r1[s, 1 - y, j].astype(jnp.float32)).astype(
+                        jnp.bfloat16
+                    )
+                else:
+                    s2[s, j] = (keep[s, j, 1 - x] + r1[s, j, 1 - x].astype(jnp.float32)).astype(
+                        jnp.bfloat16
+                    )
+            send_rs(s2.at[s], r2.at[s], 1, s, y_peer if half == 0 else x_peer)
+
+    def stage_c(k):
+        source = z if k == 0 else source_of(jnp.int32(k))
+        for half in range(2):
+            s = 2 * source + half
+            peer = y_peer if half == 0 else x_peer
+            remote(s2.at[s], r2.at[s], rs_send.at[1, s], rs_recv.at[1, s], peer).wait_recv()
+            my = x if half == 0 else y
+            for own, j in ((False, 1 - my), (True, my)):
+                if half == 0:
+                    part = keep[s, y, j] + r1[s, y, j].astype(jnp.float32)
+                else:
+                    part = keep[s, j, x] + r1[s, j, x].astype(jnp.float32)
+                part = part + r2[s, j].astype(jnp.float32)
+                if own:
+                    keep[s, y, x] = part
+                else:
+                    s3[s] = part.astype(jnp.bfloat16)
+                    send_rs(s3.at[s], r3.at[s], 2, s, x_peer if half == 0 else y_peer)
+
+    def stage_d(k):
+        source = z if k == 0 else source_of(jnp.int32(k))
+        for half in range(2):
+            s = 2 * source + half
+            peer = x_peer if half == 0 else y_peer
+            remote(s3.at[s], r3.at[s], rs_send.at[2, s], rs_recv.at[2, s], peer).wait_recv()
+            out_ref[:, columns(s)] = (keep[s, y, x] + r3[s].astype(jnp.float32)).astype(
+                jnp.bfloat16
+            )
+
+    for k in range(line):
+        stage_a(k)
+        if k >= 1:
+            stage_c(k - 1)
+        stage_b(k)
+        if k >= 1:
+            stage_d(k - 1)
+    stage_c(line - 1)
+    stage_d(line - 1)
+
+    for copy in [y_copy, oy_copy] + tok_copies + rs_copies:
+        copy.wait_send()
+
+    @pl.when(has_up)
+    def _():
+        rim_up.wait_send()
+
+    @pl.when(has_down)
+    def _():
+        rim_down.wait_send()
+
+    for s in range(2 * line):
+        for buf, ups, downs, recv in (
+            (win, in_up, in_down, in_recv), (wout, out_up, out_down, out_recv)
+        ):
+            @pl.when((s // 2 <= z) & has_up)
+            def _():
+                hop(buf, s, ups, recv, up).wait_send()
+
+            @pl.when((s // 2 >= z) & has_down)
+            def _():
+                hop(buf, s, downs, recv, down).wait_send()
+
+
+def trig_table(total):
+    half = HEAD_DIM // 2
+    freq = np.float64(ROPE_BASE) ** (-np.arange(half) / half)
+    angle = np.arange(total)[:, None] * freq
+    cosine, sine = np.cos(angle), np.sin(angle)
+    return np.concatenate([cosine, cosine, -sine, sine], axis=1).astype(np.float32)
+
+
+def fused_device(
+    tokens, norm_gain, query_weight, key_weight, value_weight, gate_weight, left_weight,
+    input_weight, query_gain, key_gain, sink_logit, conv_weight, out_attention, out_conv,
+):
+    sp_count = lax.axis_size("sp")
+    line = sp_count // 2
+    rows, width = tokens.shape
+    depth = query_weight.shape[1]
+    qr = query_weight.shape[0] // 2
+    kr = key_weight.shape[0]
+    cr = gate_weight.shape[0] // 2
+    fan = qr + 2 * kr + 3 * cr
+    plane = 8 * rows
+    dims = dict(line=line, rows=rows, depth=depth, qr=qr, kr=kr, cr=cr)
+    vm = pl.BlockSpec(memory_space=pltpu.VMEM)
+    sm = pl.BlockSpec(memory_space=pltpu.SMEM)
+    hb = pl.BlockSpec(memory_space=pl.ANY)
+    bf16, f32 = jnp.bfloat16, jnp.float32
+    dma = pltpu.SemaphoreType.DMA
+    n = sp_count
+    scratch = [
+        pltpu.VMEM((rows, width), bf16),
+        pltpu.VMEM((plane, 2 * HEAD_DIM), f32),
+        pltpu.VMEM((fan, depth), bf16),
+        pltpu.VMEM((qr + cr, depth), bf16),
+        pltpu.VMEM((n, fan, depth), bf16),
+        pltpu.VMEM((n, qr + cr, depth), bf16),
+        pltpu.VMEM((8, rows, width), bf16),
+        pltpu.VMEM((plane, fan), f32),
+        pltpu.VMEM((plane + 2 * WINDOW, qr + cr), bf16),
+        pltpu.VMEM((plane, qr + cr), bf16),
+        pltpu.VMEM((2, plane, qr), bf16),
+        pltpu.VMEM((n, 2, 2, rows, depth), f32),
+        pltpu.VMEM((n, 2, 2, rows, depth), bf16),
+        pltpu.VMEM((n, 2, 2, rows, depth), bf16),
+        pltpu.VMEM((n, 2, rows, depth), bf16),
+        pltpu.VMEM((n, 2, rows, depth), bf16),
+        pltpu.VMEM((n, rows, depth), bf16),
+        pltpu.VMEM((n, rows, depth), bf16),
+        dma((18,)), dma((1,)), dma((1,)), dma((n,)), dma((n,)),
+        dma((n,)), dma((n,)), dma((n,)), dma((n,)),
+        dma((7,)), dma((8,)), dma((2,)), dma((2,)), dma((3, n)), dma((3, n)),
+    ]
+    taps = conv_weight.reshape(3, 2, cr).transpose(1, 0, 2)
+    return pl.pallas_call(
+        functools.partial(fused_kernel, dims),
+        out_shape=jax.ShapeDtypeStruct((rows, width), bf16),
+        in_specs=[hb, vm, hb, hb, hb, hb, hb, hb, vm, vm, sm, vm, hb, hb, hb],
+        out_specs=vm,
+        scratch_shapes=scratch,
+        compiler_params=pltpu.CompilerParams(
+            collective_id=0, has_side_effects=True, vmem_limit_bytes=56 * 1024 * 1024
+        ),
+    )(
+        tokens, norm_gain[None, :], query_weight, key_weight, value_weight, gate_weight,
+        left_weight, input_weight, jnp.tile(query_gain, 2)[None, :],
+        jnp.tile(key_gain, 2)[None, :], sink_logit[None, :], taps, out_attention, out_conv,
+        jnp.asarray(trig_table(plane * line)),
+    )
+
+
+def local_device(*args):
+    tokens, query_weight, key_weight, gate_weight = args[0], args[2], args[3], args[5]
+    fits = (
+        lax.axis_size("sp") % 2 == 0
+        and lax.axis_size("sp") <= 16
+        and lax.axis_size("tp") == 4
+        and query_weight.shape[1] % 128 == 0
+        and query_weight.shape[0] == 4 * HEAD_DIM
+        and key_weight.shape[0] == HEAD_DIM
+        and gate_weight.shape[0] == 256
+        and tokens.shape[0] % 16 == 0
+        and 8 * tokens.shape[0] % BLOCK == 0
+    )
+    return fused_device(*args) if fits else per_device(*args)
+
+
 def solution(mesh):
     in_specs = (
         P(("sp", "tp"), None),
@@ -209,5 +726,5 @@
     )
     out_specs = P(("sp", "tp"), None)
     return jax.shard_map(
-        per_device, mesh=mesh, in_specs=in_specs, out_specs=out_specs, check_vma=False
-    )
+        local_device, mesh=mesh, in_specs=in_specs, out_specs=out_specs, check_vma=False
+    )

time: 309 us -> 98.8 us (0.32)
  waiting for transfers between devices: 197 us -> 0 us
  Pallas kernels: 0 us -> 95.1 us
  blocking collectives: 64.2 us -> 0 us
  matrix products: 15.3 us -> 0 us
  between operations: 13.8 us -> 0.01 us
  starting transfers between devices: 9.06 us -> 0 us
  other arithmetic: 5.49 us -> 0 us
    all_gather x7 -> x0, waiting for transfers between devices: 165 us -> none  [the longest x1 40.5 us: per_device(): lax.all_gather(out_conv, 'sp', axis=1, tiled=True)]
    pallas_call x0 -> x1, Pallas kernels: none -> 95.1 us  [fused_device(): pl.pallas_call(functools.partial(fused_kernel, dims), out_shape=jax.Shape...]
    all_gather x2 -> x0, blocking collectives: 64.2 us -> none  [the longest x1 32.9 us: per_device(): lax.all_gather(key_weight, 'sp', axis=1, tiled=True)]
    reduce_scatter x1 -> x0, waiting for transfers between devices: 24 us -> none  [per_device(): lax.psum_scatter((jnp.dot(attended, attn_out_full, preferred_element_type...]
    dot_general x11 -> x0, matrix products: 15.3 us -> none  [the longest x5 8.56 us: project(): lax.dot_general(rows, weight, (((1,), (1,)), ((), ())), preferred_element...]
    ppermute x4 -> x0, starting transfers between devices: 8.79 us -> none  [the longest x2 6.2 us: with_halo(): lax.ppermute(tail, axis, [(i, (i + 1) % count) for i in range(ends)])]
    ppermute x4 -> x0, waiting for transfers between devices: 3.96 us -> none  [the longest x2 3.95 us: with_halo(): lax.ppermute(head, axis, [((i + 1) % count, i) for i in range(ends)])]
    unnamed x8 -> x0, waiting for transfers between devices: 3.68 us -> none
  transfers between devices with their start and end apart: 12 -> 0, of which waited for: 7 -> 0; matrix products, arithmetic and copies ran while one was open for 5% -> 0% of each run, Pallas kernels for 0% -> 0%
where the time goes in v1:
time: 98.8 us; the launch traced here: 98.6 us
  Pallas kernels  95.1 us (96%)
  local copies, waits for them, and re-layouts  3.54 us (4%)
    pallas_call x1, Pallas kernels, fused_device(): pl.pallas_call(functools.partial(fused_kernel, dims), out_shape=jax.Shape...  95.1 us
    unnamed x5, local copies, waits for them, and re-layouts  2.39 us

profile of v1, /device:TPU:0, one launch (start us, length us, event | category | flops | bytes accessed | tf_op | source)
XLA Modules:
  0.0 98.6 jit_solution(2624286939069949525)
XLA Ops:
  0.0 0.0 copy-start
  0.0 0.7 copy-done
  0.7 0.0 copy-start.1
  0.7 0.6 broadcast_in_dim_tile.6.qgain_ref
  1.3 0.1 copy-done.1
  1.3 0.6 broadcast_in_dim_tile.7.kgain_ref
  1.9 95.1 %shard_map.145 = bf16[64,2048]{1,0:T(8,128)(2,1)} custom-call(bf16[64,2048]{1,0:T(8,128)(2,1)} %tok_hbm.1, f32[1,2048]{1,0:T(1,128)} %bitcast.5, bf16[256,256]{1,0:T(8,128)(2,1)} %q_hbm.1, bf16[64,256]{1,0:T(8,128)(2,1)} %k_hbm.1, bf16[64,256]{1,0:T(8,128)(2,1)} %v_hbm.1, bf16[256,256]{1,0:T(8,128)(2,1)} %g_hbm.1, bf16[256,256]{1,0:T(8,128)(2,1)} %l_hbm.1, ...), custom_call_target="tpu_custom_call" | custom-call | tf_op jit(solution)/shard_map/pallas_call | solution.py:677
  96.9 1.7 %copy.17 = bf16[64,2048]{1,0:T(8,128)(2,1)} copy(bf16[64,2048]{1,0:T(8,128)(2,1)} %shard_map.145) | data formatting | bytes 524288
  (2 shorter events, 0.0 us)
Async XLA Ops:
  0.0 0.7 copy-start
  0.7 0.7 copy-start.1

commit v2 on v1

--- a/solution.py
+++ b/solution.py
@@ -203,10 +203,12 @@
     tok_hbm, gain_ref, q_hbm, k_hbm, v_hbm, g_hbm, l_hbm, i_hbm,
     qgain_ref, kgain_ref, sink_ref, conv_ref, oa_hbm, oc_hbm, trig_hbm,
     out_ref,
-    tok, trig, stage, ostage, win, wout, normed, acc, rim, mix, qrot,
+    tok, trig, stage, ostage, win, wout, normed, normed2, acc, acc2, rim, prod, prod2, mix_a, mix_c, gated2,
+    qrot,
     keep, s1, r1, s2, r2, s3, r3,
     local_sem, y_send, oy_send, in_recv, out_recv, in_up, in_down, out_up, out_down,
-    tok_send, tok_recv, rim_send, rim_recv, rs_send, rs_recv,
+    tok_send, tok_recv, tok2_send, tok2_recv, rim_send, rim_recv, prod_send, prod_recv, g_send, g_recv,
+    rs_send, rs_recv,
 ):
     line, rows, depth, qr, kr, cr = (
         dims["line"], dims["rows"], dims["depth"], dims["qr"], dims["kr"], dims["cr"]
@@ -225,6 +227,12 @@
     s_own = sp
     s_mate = 2 * z + 1 - y
     plane = 8 * rows
+    core = qr + 2 * kr
+    is_end = (z == 0) | (z == line - 1)
+    not_end = (z > 0) & (z < line - 1)
+    is_help = (z == 1) | (z == line - 2)
+    help_dev = (jnp.where(z == 0, 2 + y, 2 * (line - 2) + y), tp)
+    end_dev = (jnp.where(z == 1, y, 2 * (line - 1) + y), tp)
 
     barrier = pltpu.get_barrier_semaphore()
     for peer in (y_peer, x_peer, c_peer):
@@ -282,6 +290,41 @@
     def hop(buf, s, send, recv, peer):
         return remote(buf.at[s], buf.at[s], send.at[s], recv.at[s], peer)
 
+    def trim_hop(s, send, peer):
+        return remote(
+            win.at[s, 0:core], win.at[s, 0:core], send.at[s], in_recv.at[s], peer
+        )
+
+    up_full = z + 1 < line - 1
+    up_trim = z + 1 == line - 1
+    down_full = z - 1 > 0
+    down_trim = z - 1 == 0
+
+    def in_sends(s, source, act):
+        for full, trim, way, send, peer in (
+            (up_full, up_trim, source <= z, in_up, up),
+            (down_full, down_trim, source >= z, in_down, down),
+        ):
+            @pl.when(way & full)
+            def _():
+                act(hop(win, s, send, in_recv, peer))
+
+            @pl.when(way & trim)
+            def _():
+                act(trim_hop(s, send, peer))
+
+    def in_forward(s, source):
+        in_sends(s, source, lambda copy: copy.start())
+
+    def in_wait(s):
+        @pl.when(is_end)
+        def _():
+            trim_hop(s, in_up, up).wait_recv()
+
+        @pl.when(not_end)
+        def _():
+            hop(win, s, in_up, in_recv, up).wait_recv()
+
     def forward(buf, s, source, ups, downs, recv):
         @pl.when((source <= z) & has_up)
         def _():
@@ -293,7 +336,7 @@
 
     for copy in mine:
         copy.wait()
-    forward(win, s_own, z, in_up, in_down, in_recv)
+    in_forward(s_own, z)
     for copy in theirs:
         copy.wait()
     y_copy = remote(stage, win.at[s_own], y_send.at[0], in_recv.at[s_own], y_peer)
@@ -303,12 +346,27 @@
     t = t * lax.rsqrt(jnp.mean(t * t, axis=-1, keepdims=True) + EPS) * gain_ref[...]
     own_block = 4 * y + 2 * x + c
     normed[own_block] = t.astype(jnp.bfloat16)
+
+    def end_tok(block, slot):
+        return remote(
+            normed.at[block], normed2.at[block], tok2_send.at[slot], tok2_recv.at[block], help_dev
+        )
+
+    def tok2_hop(block, slot, peer):
+        return remote(
+            normed2.at[block], normed2.at[block], tok2_send.at[slot], tok2_recv.at[block], peer
+        )
+
     for copy in out_theirs:
         copy.wait()
     oy_copy = remote(ostage, wout.at[s_own], oy_send.at[0], out_recv.at[s_own], y_peer)
     oy_copy.start()
     for copy in out_mine:
         copy.wait()
+
+    @pl.when(is_end)
+    def _():
+        end_tok(own_block, 0).start()
 
     def block_of(yy, xx, cc):
         return 4 * yy + 2 * xx + cc
@@ -339,7 +397,7 @@
     tok_copies += more
 
     hop(win, s_mate, in_up, in_recv, up).wait_recv()
-    forward(win, s_mate, z, in_up, in_down, in_recv)
+    in_forward(s_mate, z)
     hop(wout, s_mate, out_up, out_recv, up).wait_recv()
 
     def own_out(flag_up, flag_down):
@@ -352,9 +410,13 @@
             def _():
                 hop(wout, s, out_down, out_recv, down).start()
 
+    tok_wait(yb0)
+
+    @pl.when(is_end)
+    def _():
+        end_tok(yb0, 1).start()
+
     own_out(z == 0, z == line - 1)
-
-    tok_wait(yb0)
     copy = tok_hop(yb0, 5, c_peer)
     copy.start()
     tok_copies.append(copy)
@@ -369,11 +431,18 @@
     def columns(s):
         return pl.ds(pl.multiple_of(s * depth, depth), depth)
 
-    def in_dot(s):
+    def dot_t(a, w):
+        return lax.dot_general(a, w, (((1,), (1,)), ((), ())), preferred_element_type=jnp.float32)
+
+    def in_dot(s, first):
         a = normed[:, :, columns(s)].reshape(plane, depth)
-        return lax.dot_general(
-            a, win[s], (((1,), (1,)), ((), ())), preferred_element_type=jnp.float32
-        )
+        low_part = dot_t(a, win[s, 0:core])
+        acc[:, 0:core] = low_part if first else acc[:, 0:core] + low_part
+
+        @pl.when(not_end)
+        def _():
+            high_part = dot_t(a, win[s, core:])
+            acc[:, core:] = high_part if first else acc[:, core:] + high_part
 
     paired = jnp.minimum(z, line - 1 - z)
     below_longer = z > line - 1 - z
@@ -383,19 +452,26 @@
         below = jnp.where(k <= 2 * paired, k % 2 == 1, below_longer)
         return jnp.where(below, z - d, z + d)
 
-    acc[...] = in_dot(s_own)
-    acc[...] += in_dot(s_mate)
+    in_dot(s_own, True)
+    in_dot(s_mate, False)
 
     def in_step(k, carry):
         source = source_of(k)
+        for turn, block, slot in ((2, own_block, 2), (line - 1, yb0, 4)):
+            @pl.when(is_help & (k == turn))
+            def _():
+                tok2_hop(block, slot, end_dev).wait_recv()
+                tok2_hop(block, slot, x_peer).start()
+                tok2_hop(block, slot + 1, c_peer).start()
+
         for half in range(2):
             first = jnp.where(half == 0, y, 1 - y)
             s = 2 * source + first
-            hop(win, s, in_up, in_recv, up).wait_recv()
-            forward(win, s, source, in_up, in_down, in_recv)
+            in_wait(s)
+            in_forward(s, source)
             if half == 1:
                 own_out(source == 0, source == line - 1)
-            acc[...] += in_dot(s)
+            in_dot(s, False)
         return carry
 
     lax.fori_loop(1, line, in_step, 0)
@@ -420,19 +496,18 @@
 
     kv = bf(acc[:, qr : 2 * qr])
     ksq = jnp.sum(jnp.where(low, kv * kv, 0.0), axis=-1, keepdims=True) / HEAD_DIM
-    kn = kv * lax.rsqrt(ksq + EPS) * kgain_ref[...]
+    kgain = jnp.concatenate([kgain_ref[...], kgain_ref[...]], axis=1)
+    kn = kv * lax.rsqrt(ksq + EPS) * kgain
     krot = rot(kn)
-    rim[WINDOW : WINDOW + plane, 0:qr] = jnp.where(low, krot, kv).astype(jnp.bfloat16)
+    rim[WINDOW : WINDOW + plane, :] = jnp.where(low, krot, kv).astype(jnp.bfloat16)
     base = 2 * qr
-    left = bf(acc[:, base + cr : base + 2 * cr])
-    inputs = bf(acc[:, base + 2 * cr : base + 3 * cr])
-    rim[WINDOW : WINDOW + plane, qr : qr + cr] = (left * inputs).astype(jnp.bfloat16)
 
     qv = bf(acc[:, 0:qr])
     qq = qv * qv
     q_lo = jnp.sum(jnp.where(low, qq, 0.0), axis=-1, keepdims=True) / HEAD_DIM
     q_hi = jnp.sum(jnp.where(low, 0.0, qq), axis=-1, keepdims=True) / HEAD_DIM
-    qn = qv * lax.rsqrt(jnp.where(low, q_lo, q_hi) + EPS) * qgain_ref[...]
+    qgain = jnp.concatenate([qgain_ref[...], qgain_ref[...]], axis=1)
+    qn = qv * lax.rsqrt(jnp.where(low, q_lo, q_hi) + EPS) * qgain
     qro = rot(qn)
 
     bottom = pl.ds(WINDOW, WINDOW)
@@ -450,7 +525,7 @@
     def _():
         rim_down.start()
 
-    zero_rim = jnp.zeros((WINDOW, qr + cr), jnp.bfloat16)
+    zero_rim = jnp.zeros((WINDOW, qr), jnp.bfloat16)
 
     @pl.when(z == 0)
     def _():
@@ -463,6 +538,90 @@
     qrot[0] = jnp.where(low, qro, 0.0).astype(jnp.bfloat16)
     qrot[1] = jnp.where(low, pltpu.roll(qro, HEAD_DIM, 1), 0.0).astype(jnp.bfloat16)
 
+    pad = 16
+    zero_pad = jnp.zeros((pad, cr), jnp.bfloat16)
+    taps = conv_ref[y]
+
+    def convolve(ref, gate):
+        p = ref[...].astype(jnp.float32)
+        before = pltpu.roll(p, 1, 0)[pad : pad + plane]
+        after = pltpu.roll(p, plane + 2 * pad - 1, 0)[pad : pad + plane]
+        mixed = taps[0:1] * before + taps[1:2] * p[pad : pad + plane] + taps[2:3] * after
+        return (gate * mixed).astype(jnp.bfloat16)
+
+    prod_up = remote(
+        prod.at[pl.ds(plane, pad)], prod.at[pl.ds(0, pad)], prod_send.at[0], prod_recv.at[0], up
+    )
+    prod_down = remote(
+        prod.at[pl.ds(pad, pad)], prod.at[pl.ds(pad + plane, pad)],
+        prod_send.at[1], prod_recv.at[1], down,
+    )
+    from_up = not_end & up_full
+    from_down = not_end & down_full
+
+    @pl.when(not_end)
+    def _():
+        left = bf(acc[:, base + cr : base + 2 * cr])
+        inputs = bf(acc[:, base + 2 * cr : base + 3 * cr])
+        prod[pad : pad + plane] = (left * inputs).astype(jnp.bfloat16)
+
+    @pl.when(from_up)
+    def _():
+        prod_up.start()
+
+    @pl.when(from_down)
+    def _():
+        prod_down.start()
+
+    g_copy = remote(gated2, mix_c, g_send.at[0], g_recv.at[0], end_dev)
+
+    @pl.when(is_help)
+    def _():
+        for block, slot in ((xb, 6), (yb1, 7)):
+            tok2_hop(block, slot, x_peer).wait_recv()
+            tok2_hop(block, slot, c_peer).start()
+        for yy in range(2):
+            for xx in range(2):
+                tok2_hop(block_of(yy, xx, 1 - c), 0, c_peer).wait_recv()
+        acc2[...] = jnp.zeros_like(acc2)
+
+        def help_step(s, carry):
+            a = normed2[:, :, columns(s)].reshape(plane, depth)
+            acc2[...] += dot_t(a, win[s, core:])
+            return carry
+
+        lax.fori_loop(0, 2 * line, help_step, 0)
+        prod2[pad : pad + plane] = (
+            bf(acc2[:, cr : 2 * cr]) * bf(acc2[:, 2 * cr : 3 * cr])
+        ).astype(jnp.bfloat16)
+
+        @pl.when(z == 1)
+        def _():
+            prod2[0:pad] = zero_pad
+            prod2[pad + plane :] = prod[pad : 2 * pad]
+            prod[0:pad] = prod2[plane : plane + pad]
+
+        @pl.when(z != 1)
+        def _():
+            prod2[0:pad] = prod[plane : plane + pad]
+            prod2[pad + plane :] = zero_pad
+            prod[pad + plane :] = prod2[pad : 2 * pad]
+
+        gated2[...] = convolve(prod2, bf(acc2[:, 0:cr]))
+        g_copy.start()
+
+    @pl.when(from_up)
+    def _():
+        prod_down.wait_recv()
+
+    @pl.when(from_down)
+    def _():
+        prod_up.wait_recv()
+
+    @pl.when(not_end)
+    def _():
+        mix_c[...] = convolve(prod, bf(acc[:, base : base + cr]))
+
     @pl.when(has_down)
     def _():
         rim_up.wait_recv()
@@ -476,7 +635,7 @@
 
     def att_step(block, carry):
         begin = pl.multiple_of(block * BLOCK, BLOCK)
-        kvb = rim[pl.ds(begin, span), 0:qr]
+        kvb = rim[pl.ds(begin, span), :]
         qb = qrot[:, pl.ds(begin, BLOCK), :].reshape(2 * BLOCK, qr)
         scores = lax.dot_general(
             qb, kvb, (((1,), (1,)), ((), ())), preferred_element_type=jnp.float32
@@ -496,24 +655,18 @@
         o = jnp.dot(weights, kvb, preferred_element_type=jnp.float32)
         low_b = lax.broadcasted_iota(jnp.int32, (BLOCK, qr), 1) < HEAD_DIM
         both = jnp.where(low_b, pltpu.roll(o[:BLOCK], HEAD_DIM, 1), o[BLOCK:])
-        mix[pl.ds(begin, BLOCK), 0:qr] = both.astype(jnp.bfloat16)
+        mix_a[pl.ds(begin, BLOCK), :] = both.astype(jnp.bfloat16)
         return carry
 
     lax.fori_loop(0, plane // BLOCK, att_step, 0)
 
-    extra = plane + 32
-    p = rim[WINDOW - 16 : WINDOW + plane + 16, qr : qr + cr].astype(jnp.float32)
-    taps = conv_ref[y]
-    before = pltpu.roll(p, 1, 0)[16 : 16 + plane]
-    after = pltpu.roll(p, extra - 1, 0)[16 : 16 + plane]
-    convolved = taps[0:1] * before + taps[1:2] * p[16 : 16 + plane] + taps[2:3] * after
-    gate = bf(acc[:, base : base + cr])
-    mix[:, qr : qr + cr] = (gate * convolved).astype(jnp.bfloat16)
+    @pl.when(is_end)
+    def _():
+        g_copy.wait_recv()
 
     def group(cc):
-        return [
-            mix[pl.ds(pl.multiple_of((2 * q + cc) * rows, rows), rows), :] for q in range(4)
-        ]
+        spans = [pl.ds(pl.multiple_of((2 * q + cc) * rows, rows), rows) for q in range(4)]
+        return [jnp.concatenate([mix_a[w, :], mix_c[w, :]], axis=1) for w in spans]
 
     mine_rows = jnp.concatenate(group(c), axis=0)
     other_rows = jnp.concatenate(group(1 - c), axis=0)
@@ -609,17 +762,35 @@
     def _():
         rim_down.wait_send()
 
+    @pl.when(is_end)
+    def _():
+        end_tok(own_block, 0).wait_send()
+        end_tok(yb0, 1).wait_send()
+
+    @pl.when(is_help)
+    def _():
+        for slot in range(2, 8):
+            tok2_hop(own_block, slot, x_peer).wait_send()
+        g_copy.wait_send()
+
+    @pl.when(from_up)
+    def _():
+        prod_up.wait_send()
+
+    @pl.when(from_down)
+    def _():
+        prod_down.wait_send()
+
     for s in range(2 * line):
-        for buf, ups, downs, recv in (
-            (win, in_up, in_down, in_recv), (wout, out_up, out_down, out_recv)
-        ):
-            @pl.when((s // 2 <= z) & has_up)
-            def _():
-                hop(buf, s, ups, recv, up).wait_send()
-
-            @pl.when((s // 2 >= z) & has_down)
-            def _():
-                hop(buf, s, downs, recv, down).wait_send()
+        in_sends(s, s // 2, lambda copy: copy.wait_send())
+
+        @pl.when((s // 2 <= z) & has_up)
+        def _():
+            hop(wout, s, out_up, out_recv, up).wait_send()
+
+        @pl.when((s // 2 >= z) & has_down)
+        def _():
+            hop(wout, s, out_down, out_recv, down).wait_send()
 
 
 def trig_table(total):
@@ -658,9 +829,15 @@
         pltpu.VMEM((n, fan, depth), bf16),
         pltpu.VMEM((n, qr + cr, depth), bf16),
         pltpu.VMEM((8, rows, width), bf16),
+        pltpu.VMEM((8, rows, width), bf16),
         pltpu.VMEM((plane, fan), f32),
-        pltpu.VMEM((plane + 2 * WINDOW, qr + cr), bf16),
-        pltpu.VMEM((plane, qr + cr), bf16),
+        pltpu.VMEM((plane, 3 * cr), f32),
+        pltpu.VMEM((plane + 2 * WINDOW, qr), bf16),
+        pltpu.VMEM((plane + 32, cr), bf16),
+        pltpu.VMEM((plane + 32, cr), bf16),
+        pltpu.VMEM((plane, qr), bf16),
+        pltpu.VMEM((plane, cr), bf16),
+        pltpu.VMEM((plane, cr), bf16),
         pltpu.VMEM((2, plane, qr), bf16),
         pltpu.VMEM((n, 2, 2, rows, depth), f32),
         pltpu.VMEM((n, 2, 2, rows, depth), bf16),
@@ -671,7 +848,8 @@
         pltpu.VMEM((n, rows, depth), bf16),
         dma((18,)), dma((1,)), dma((1,)), dma((n,)), dma((n,)),
         dma((n,)), dma((n,)), dma((n,)), dma((n,)),
-        dma((7,)), dma((8,)), dma((2,)), dma((2,)), dma((3, n)), dma((3, n)),
+        dma((7,)), dma((8,)), dma((8,)), dma((8,)), dma((2,)), dma((2,)), dma((2,)), dma((2,)),
+        dma((1,)), dma((1,)), dma((3, n)), dma((3, n)),
     ]
     taps = conv_weight.reshape(3, 2, cr).transpose(1, 0, 2)
     return pl.pallas_call(
@@ -685,8 +863,8 @@
         ),
     )(
         tokens, norm_gain[None, :], query_weight, key_weight, value_weight, gate_weight,
-        left_weight, input_weight, jnp.tile(query_gain, 2)[None, :],
-        jnp.tile(key_gain, 2)[None, :], sink_logit[None, :], taps, out_attention, out_conv,
+        left_weight, input_weight, query_gain[None, :],
+        key_gain[None, :], sink_logit[None, :], taps, out_attention, out_conv,
         jnp.asarray(trig_table(plane * line)),
     )
 
@@ -695,7 +873,7 @@
     tokens, query_weight, key_weight, gate_weight = args[0], args[2], args[3], args[5]
     fits = (
         lax.axis_size("sp") % 2 == 0
-        and lax.axis_size("sp") <= 16
+        and 8 <= lax.axis_size("sp") <= 16
         and lax.axis_size("tp") == 4
         and query_weight.shape[1] % 128 == 0
         and query_weight.shape[0] == 4 * HEAD_DIM

time: 98.8 us -> 89.2 us (0.903)
  Pallas kernels: 95.1 us -> 87.4 us
  local copies, waits for them, and re-layouts: 3.54 us -> 1.67 us
    pallas_call x1, Pallas kernels: 95.1 us -> 87.4 us  [fused_device(): pl.pallas_call(functools.partial(fused_kernel, dims), out_shape=jax.Shape...]
    another operation x4 -> x0, local copies, waits for them, and re-layouts: 1.16 us -> none  [the longest x2 0.59 us: fused_device(): jnp.tile(query_gain, 2)[None, :]]
    unnamed x5 -> x1, local copies, waits for them, and re-layouts: 2.39 us -> 1.67 us
where the time goes in v2:
time: 89.2 us; the launch traced here: 89 us
  Pallas kernels  87.4 us (98%)
  local copies, waits for them, and re-layouts  1.67 us (2%)
    pallas_call x1, Pallas kernels, fused_device(): pl.pallas_call(functools.partial(fused_kernel, dims), out_shape=jax.Shape...  87.4 us

profile of v2, /device:TPU:0, one launch (start us, length us, event | category | flops | bytes accessed | tf_op | source)
XLA Modules:
  0.0 89.0 jit_solution(8828779261488494262)
XLA Ops:
  0.0 87.4 %shard_map.145 = bf16[64,2048]{1,0:T(8,128)(2,1)} custom-call(bf16[64,2048]{1,0:T(8,128)(2,1)} %tok_hbm.1, f32[1,2048]{1,0:T(1,128)} %bitcast.7, bf16[256,256]{1,0:T(8,128)(2,1)} %q_hbm.1, bf16[64,256]{1,0:T(8,128)(2,1)} %k_hbm.1, bf16[64,256]{1,0:T(8,128)(2,1)} %v_hbm.1, bf16[256,256]{1,0:T(8,128)(2,1)} %g_hbm.1, bf16[256,256]{1,0:T(8,128)(2,1)} %l_hbm.1, ...), custom_call_target="tpu_custom_call" | custom-call | tf_op jit(solution)/shard_map/pallas_call | solution.py:855
  87.4 1.7 %copy.17 = bf16[64,2048]{1,0:T(8,128)(2,1)} copy(bf16[64,2048]{1,0:T(8,128)(2,1)} %shard_map.145) | data formatting | bytes 524288

commit v3 on v2

--- a/solution.py
+++ b/solution.py
@@ -290,40 +290,28 @@
     def hop(buf, s, send, recv, peer):
         return remote(buf.at[s], buf.at[s], send.at[s], recv.at[s], peer)
 
-    def trim_hop(s, send, peer):
+    chunks = ((0, core), (core, core + 3 * cr))
+
+    def in_hop(s, part, send, peer):
+        lo, hi = chunks[part]
         return remote(
-            win.at[s, 0:core], win.at[s, 0:core], send.at[s], in_recv.at[s], peer
+            win.at[s, lo:hi], win.at[s, lo:hi], send.at[part, s], in_recv.at[part, s], peer
         )
 
+    def in_sends(s, source, part, act):
+        for inner, edge, way, send, peer in (
+            (z + 1 < line - 1, has_up, source <= z, in_up, up),
+            (z - 1 > 0, has_down, source >= z, in_down, down),
+        ):
+            @pl.when(way & (edge if part == 0 else inner))
+            def _():
+                act(in_hop(s, part, send, peer))
+
+    def in_forward(s, source, part):
+        in_sends(s, source, part, lambda copy: copy.start())
+
     up_full = z + 1 < line - 1
-    up_trim = z + 1 == line - 1
     down_full = z - 1 > 0
-    down_trim = z - 1 == 0
-
-    def in_sends(s, source, act):
-        for full, trim, way, send, peer in (
-            (up_full, up_trim, source <= z, in_up, up),
-            (down_full, down_trim, source >= z, in_down, down),
-        ):
-            @pl.when(way & full)
-            def _():
-                act(hop(win, s, send, in_recv, peer))
-
-            @pl.when(way & trim)
-            def _():
-                act(trim_hop(s, send, peer))
-
-    def in_forward(s, source):
-        in_sends(s, source, lambda copy: copy.start())
-
-    def in_wait(s):
-        @pl.when(is_end)
-        def _():
-            trim_hop(s, in_up, up).wait_recv()
-
-        @pl.when(not_end)
-        def _():
-            hop(win, s, in_up, in_recv, up).wait_recv()
 
     def forward(buf, s, source, ups, downs, recv):
         @pl.when((source <= z) & has_up)
@@ -336,11 +324,18 @@
 
     for copy in mine:
         copy.wait()
-    in_forward(s_own, z)
+    for part in range(2):
+        in_forward(s_own, z, part)
     for copy in theirs:
         copy.wait()
-    y_copy = remote(stage, win.at[s_own], y_send.at[0], in_recv.at[s_own], y_peer)
-    y_copy.start()
+    y_copies = [
+        remote(
+            stage.at[lo:hi], win.at[s_own, lo:hi], y_send.at[part], in_recv.at[part, s_own], y_peer
+        )
+        for part, (lo, hi) in enumerate(chunks)
+    ]
+    for copy in y_copies:
+        copy.start()
     tok_copy.wait()
     t = tok[...].astype(jnp.float32)
     t = t * lax.rsqrt(jnp.mean(t * t, axis=-1, keepdims=True) + EPS) * gain_ref[...]
@@ -387,6 +382,10 @@
     for copy in tok_copies:
         copy.start()
 
+    for part in range(2):
+        in_hop(s_mate, part, in_up, up).wait_recv()
+        in_forward(s_mate, z, part)
+
     def tok_wait(block):
         tok_hop(block, 0, x_peer).wait_recv()
 
@@ -396,8 +395,6 @@
         copy.start()
     tok_copies += more
 
-    hop(win, s_mate, in_up, in_recv, up).wait_recv()
-    in_forward(s_mate, z)
     hop(wout, s_mate, out_up, out_recv, up).wait_recv()
 
     def own_out(flag_up, flag_down):
@@ -467,8 +464,14 @@
         for half in range(2):
             first = jnp.where(half == 0, y, 1 - y)
             s = 2 * source + first
-            in_wait(s)
-            in_forward(s, source)
+            in_hop(s, 0, in_up, up).wait_recv()
+            in_forward(s, source, 0)
+
+            @pl.when(not_end)
+            def _():
+                in_hop(s, 1, in_up, up).wait_recv()
+                in_forward(s, source, 1)
+
             if half == 1:
                 own_out(source == 0, source == line - 1)
             in_dot(s, False)
@@ -573,6 +576,19 @@
     def _():
         prod_down.start()
 
+    def out_take(k):
+        source = source_of(jnp.int32(k))
+        for half in range(2):
+            s = 2 * source + half
+            hop(wout, s, out_up, out_recv, up).wait_recv()
+            forward(wout, s, source, out_up, out_down, out_recv)
+
+    def inner_take(k):
+        @pl.when(not_end)
+        def _():
+            out_take(k)
+
+    inner_take(1)
     g_copy = remote(gated2, mix_c, g_send.at[0], g_recv.at[0], end_dev)
 
     @pl.when(is_help)
@@ -621,6 +637,9 @@
     @pl.when(not_end)
     def _():
         mix_c[...] = convolve(prod, bf(acc[:, base : base + cr]))
+
+    for k in range(2, line - 1):
+        inner_take(k)
 
     @pl.when(has_down)
     def _():
@@ -679,11 +698,13 @@
 
     def stage_a(k):
         source = z if k == 0 else source_of(jnp.int32(k))
+        if k:
+            @pl.when(is_end)
+            def _():
+                out_take(k)
+
         for half in range(2):
             s = 2 * source + half
-            if k:
-                hop(wout, s, out_up, out_recv, up).wait_recv()
-                forward(wout, s, source, out_up, out_down, out_recv)
             weight = wout[s]
             s1[s] = jnp.dot(
                 other_rows, weight, preferred_element_type=jnp.float32
@@ -741,17 +762,14 @@
                 jnp.bfloat16
             )
 
-    for k in range(line):
-        stage_a(k)
-        if k >= 1:
-            stage_c(k - 1)
-        stage_b(k)
-        if k >= 1:
-            stage_d(k - 1)
-    stage_c(line - 1)
-    stage_d(line - 1)
-
-    for copy in [y_copy, oy_copy] + tok_copies + rs_copies:
+    for k in range(line + 3):
+        if k == line - 1:
+            inner_take(k)
+        for late, step in enumerate((stage_a, stage_b, stage_c, stage_d)):
+            if 0 <= k - late < line:
+                step(k - late)
+
+    for copy in y_copies + [oy_copy] + tok_copies + rs_copies:
         copy.wait_send()
 
     @pl.when(has_up)
@@ -782,7 +800,8 @@
         prod_down.wait_send()
 
     for s in range(2 * line):
-        in_sends(s, s // 2, lambda copy: copy.wait_send())
+        for part in range(2):
+            in_sends(s, s // 2, part, lambda copy: copy.wait_send())
 
         @pl.when((s // 2 <= z) & has_up)
         def _():
@@ -846,8 +865,8 @@
         pltpu.VMEM((n, 2, rows, depth), bf16),
         pltpu.VMEM((n, rows, depth), bf16),
         pltpu.VMEM((n, rows, depth), bf16),
-        dma((18,)), dma((1,)), dma((1,)), dma((n,)), dma((n,)),
-        dma((n,)), dma((n,)), dma((n,)), dma((n,)),
+        dma((18,)), dma((2,)), dma((1,)), dma((2, n)), dma((n,)),
+        dma((2, n)), dma((2, n)), dma((n,)), dma((n,)),
         dma((7,)), dma((8,)), dma((8,)), dma((8,)), dma((2,)), dma((2,)), dma((2,)), dma((2,)),
         dma((1,)), dma((1,)), dma((3, n)), dma((3, n)),
     ]

time: 89.2 us -> 82.8 us (0.928)
  Pallas kernels: 87.4 us -> 80.9 us
    pallas_call x1, Pallas kernels: 87.4 us -> 80.9 us  [fused_device(): pl.pallas_call(functools.partial(fused_kernel, dims), out_shape=jax.Shape...]
where the time goes in v3:
time: 82.8 us; the launch traced here: 82.6 us
  Pallas kernels  80.9 us (98%)
  local copies, waits for them, and re-layouts  1.67 us (2%)
    pallas_call x1, Pallas kernels, fused_device(): pl.pallas_call(functools.partial(fused_kernel, dims), out_shape=jax.Shape...  80.9 us
    unnamed x1, local copies, waits for them, and re-layouts  1.67 us

profile of v3, /device:TPU:0, one launch (start us, length us, event | category | flops | bytes accessed | tf_op | source)
XLA Modules:
  0.0 82.6 jit_solution(4938804896205299164)
XLA Ops:
  0.0 80.9 %shard_map.145 = bf16[64,2048]{1,0:T(8,128)(2,1)} custom-call(bf16[64,2048]{1,0:T(8,128)(2,1)} %tok_hbm.1, f32[1,2048]{1,0:T(1,128)} %bitcast.7, bf16[256,256]{1,0:T(8,128)(2,1)} %q_hbm.1, bf16[64,256]{1,0:T(8,128)(2,1)} %k_hbm.1, bf16[64,256]{1,0:T(8,128)(2,1)} %v_hbm.1, bf16[256,256]{1,0:T(8,128)(2,1)} %g_hbm.1, bf16[256,256]{1,0:T(8,128)(2,1)} %l_hbm.1, ...), custom_call_target="tpu_custom_call" | custom-call | tf_op jit(solution)/shard_map/pallas_call | solution.py:874
  80.9 1.7 %copy.17 = bf16[64,2048]{1,0:T(8,128)(2,1)} copy(bf16[64,2048]{1,0:T(8,128)(2,1)} %shard_map.145) | data formatting | bytes 524288
